TPU v7x, 32 devices: a whole 2x2x4 slice. The times are simulated.
32 devices in a mesh: fs: 16 (over z, y, x), tp: 2 (over core).
Axes of the slice: x: 2, y: 2, z: 4, core: 2. Of those that a mesh axis runs over, the one named last changes fastest.
Arguments:
- tokens: bfloat16 [8192, 2048], P('fs', 'tp'), may hold values from -6 to 6
- norm_gain: bfloat16 [2048], P('tp'), may hold values from 0.099609375 to 1.8984375
- proj_u: bfloat16 [2048, 2048], P('fs', 'tp'), may hold values from -0.125 to 0.125
- proj_v: bfloat16 [2048, 2048], P('fs', 'tp'), may hold values from -0.125 to 0.125
- layer_gain: bfloat16 [2048], P('tp'), may hold values from 0.099609375 to 1.8984375
- layer_shift: bfloat16 [2048], P('tp'), may hold values from -3 to 3
- mix_weight: bfloat16 [16, 128, 128], P('tp'), may hold values from -0.5 to 0.5
- mix_bias: bfloat16 [16, 128], P('tp'), may hold values from 0.099609375 to 1.8984375
- proj_out: bfloat16 [2048, 2048], P('tp', 'fs'), may hold values from -0.1875 to 0.1875
- ffn_gain: bfloat16 [2048], P('tp'), may hold values from 0.099609375 to 1.8984375
- ffn_gate: bfloat16 [2048, 4096], P('fs', 'tp'), may hold values from -0.125 to 0.125
- ffn_value: bfloat16 [2048, 4096], P('fs', 'tp'), may hold values from -0.125 to 0.125
- conv_gate: bfloat16 [3, 4096], P(None, 'tp'), may hold values from -3 to 3
- conv_value: bfloat16 [3, 4096], P(None, 'tp'), may hold values from -3 to 3
- proj_down: bfloat16 [4096, 2048], P('tp', 'fs'), may hold values from -0.125 to 0.125
Outputs:
- result: bfloat16 [8192, 2048], P('fs', 'tp')
All inputs are finite; a program needn't handle non-finite values.
Results may differ from a plain program's by a relative error of at most 0.017.
Values may be sent and summed in bfloat16 or wider, within the bound.
A program may use at most 64 MiB of HBM per device.

v0:
```python
import jax
import jax.numpy as jnp
from jax import lax
from jax.sharding import PartitionSpec as P

GROUP_DIM = 128
BLOCK = 128
SEGMENT = 64
KERNEL = 3
SEQ_LEN = 256
EPS = 1e-06


def matmul(operand, matrix):
    return jnp.dot(operand, matrix, preferred_element_type=jnp.float32)


def local_rms(values_in, gain_row):
    values = values_in.astype(jnp.float32)
    scale_row = lax.rsqrt(jnp.mean(values * values, axis=1, keepdims=True) + EPS)
    return (values * scale_row * gain_row.astype(jnp.float32)).astype(jnp.bfloat16)


def causal_taps(values, weights):
    seq_count = values.shape[0] // SEQ_LEN
    shaped = values.reshape(seq_count, SEQ_LEN, values.shape[1])
    padded = jnp.pad(shaped, ((0, 0), (KERNEL - 1, 0), (0, 0)))
    summed = jnp.zeros(shaped.shape, jnp.float32)
    for tap_index in range(KERNEL):
        summed = summed + padded[:, tap_index : tap_index + SEQ_LEN].astype(jnp.float32) * weights[
            tap_index
        ].astype(jnp.float32)
    return summed.reshape(values.shape[0], values.shape[1])


def on_device(
    tokens,
    norm_gain,
    proj_u,
    proj_v,
    layer_gain,
    layer_shift,
    mix_weight,
    mix_bias,
    proj_out,
    ffn_gain,
    ffn_gate,
    ffn_value,
    conv_gate,
    conv_value,
    proj_down,
):
    own_width = tokens.shape[1]
    whole_tokens, whole_gain, whole_ffn_gain = (
        lax.all_gather(tokens, "tp", axis=1, tiled=True),
        lax.all_gather(norm_gain, "tp", axis=0, tiled=True),
        lax.all_gather(ffn_gain, "tp", axis=0, tiled=True),
    )
    normed = local_rms(whole_tokens, whole_gain)
    row_count = normed.shape[0]
    whole_u, whole_v = (
        lax.all_gather(proj_u, "fs", axis=0, tiled=True),
        lax.all_gather(proj_v, "fs", axis=0, tiled=True),
    )
    pre_u = matmul(normed, whole_u)
    pre_v = matmul(normed, whole_v)
    act_u = jax.nn.gelu(pre_u, approximate=False)
    act_v = jax.nn.gelu(pre_v, approximate=False)
    full_width = act_v.shape[1] * lax.axis_size("tp")
    total_sum, second = lax.psum((jnp.sum(act_v, axis=1), jnp.sum(act_v * act_v, axis=1)), "tp")
    center = total_sum / full_width
    spread = second / full_width - center * center
    mixed_in = (
        (act_v - center[:, None])
        * lax.rsqrt(spread + EPS)[:, None]
        * layer_gain.astype(jnp.float32)
        + layer_shift.astype(jnp.float32)
    ).astype(jnp.bfloat16)
    groups = mixed_in.shape[1] // GROUP_DIM
    blocks = mixed_in.reshape(row_count // BLOCK, BLOCK, groups, GROUP_DIM)
    segment = jnp.arange(BLOCK) // SEGMENT
    visible = segment[None, :] <= segment[:, None]
    masked = jnp.where(visible[None], mix_weight, jnp.zeros_like(mix_weight))
    spatial = (
        jnp.einsum("gij,njgc->nigc", masked, blocks, preferred_element_type=jnp.float32)
        + mix_bias.astype(jnp.float32).T[None, :, :, None]
    )
    gated_rows = (act_u * spatial.reshape(row_count, mixed_in.shape[1])).astype(jnp.bfloat16)
    whole_out = lax.all_gather(proj_out, "fs", axis=1, tiled=True)
    partial_value = matmul(gated_rows, whole_out)
    summed = lax.psum(partial_value.astype(jnp.bfloat16), "tp").astype(jnp.float32)
    stream_rows = (whole_tokens.astype(jnp.float32) + summed).astype(jnp.bfloat16)
    normed_two = local_rms(stream_rows, whole_ffn_gain)
    stream = lax.dynamic_slice_in_dim(stream_rows, lax.axis_index("tp") * own_width, own_width, 1)
    whole_gate, whole_value = (
        lax.all_gather(ffn_gate, "fs", axis=0, tiled=True),
        lax.all_gather(ffn_value, "fs", axis=0, tiled=True),
    )
    pre_gate = matmul(normed_two, whole_gate)
    pre_value = matmul(normed_two, whole_value)
    conv_g = causal_taps(pre_gate.astype(jnp.bfloat16), conv_gate)
    conv_v = causal_taps(pre_value.astype(jnp.bfloat16), conv_value)
    hidden = (jax.nn.silu(conv_g) * conv_v).astype(jnp.bfloat16)
    whole_down = lax.all_gather(proj_down, "fs", axis=1, tiled=True)
    partial_two = matmul(hidden, whole_down)
    return (
        stream.astype(jnp.float32)
        + lax.psum_scatter(
            partial_two.astype(jnp.bfloat16), "tp", scatter_dimension=1, tiled=True
        ).astype(jnp.float32)
    ).astype(jnp.bfloat16)


def solution(mesh):
    in_specs = (
        P("fs", "tp"),
        P("tp"),
        P("fs", "tp"),
        P("fs", "tp"),
        P("tp"),
        P("tp"),
        P("tp", None, None),
        P("tp", None),
        P("tp", "fs"),
        P("tp"),
        P("fs", "tp"),
        P("fs", "tp"),
        P(None, "tp"),
        P(None, "tp"),
        P("tp", "fs"),
    )
    out_specs = P("fs", "tp")
    return jax.shard_map(
        on_device, mesh=mesh, in_specs=in_specs, out_specs=out_specs, check_vma=False
    )
```

profile of v0, /device:TPU:0, one launch (start us, length us, event | category | flops | bytes accessed | tf_op | source)
XLA Modules:
  0.0 702.0 jit_solution(10624210363305999877)
XLA Ops:
  9.4 2.1 all_gather.28
  13.6 8.6 %all-gather.8.cloned.1.call-done = bf16[512,2048]{1,0:T(8,128)(2,1)} async-done(((bf16[512,1024]{1,0:T(8,128)(2,1)}), bf16[512,2048]{1,0:T(8,128)(2,1)}) %all-gather.8.cloned.1.call-update) | async-done | bytes 2097168 | tf_op jit(solution)/shard_map/all_gather | solution.py:55
  22.2 2.2 fusion.3
  24.4 77.3 %all-gather.12.cloned.1.call-done = bf16[2048,1024]{1,0:T(8,128)(2,1)} async-done(((bf16[128,1024]{1,0:T(8,128)(2,1)}), bf16[2048,1024]{1,0:T(8,128)(2,1)}) %all-gather.12.cloned.1.call-update) | async-done | bytes 4194320 | tf_op jit(solution)/shard_map/all_gather | solution.py:63
  101.8 9.6 %fusion.111 = (f32[512]{0:T(512)S(1)}, f32[512]{0:T(512)S(1)}, f32[512,1024]{1,0:T(8,128)}) fusion(bf16[2048,1024]{1,0:T(8,128)(2,1)} %all-gather.12.cloned.1.call-done, bf16[512,2048]{1,0:T(8,128)(2,1)S(1)} %copy-done, f32[2048]{0:T(1024)S(1)} %convert_element_type.144, f32[512]{0:T(512)S(1)} %add_rsqrt_fusion.2), kind=kOutput, calls=%fused_computation.152 | convolution fusion | flops 2186804224 | bytes 8402944 | tf_op jit(solution)/shard_map/dot_general | solution.py:15
  111.4 2.6 all-reduce.2
  114.1 2.1 fusion.32
  118.3 2.9 copy.19
  121.2 57.5 %all-gather.10.cloned.1.call-done = bf16[2048,1024]{1,0:T(8,128)(2,1)} async-done(((bf16[128,1024]{1,0:T(8,128)(2,1)}), bf16[2048,1024]{1,0:T(8,128)(2,1)}) %all-gather.10.cloned.1.call-update) | async-done | bytes 4194320 | tf_op jit(solution)/shard_map/all_gather | solution.py:62
  178.8 89.9 %all-gather.14.cloned.1.call-done = bf16[1024,2048]{1,0:T(8,128)(2,1)} async-done(((bf16[1024,128]{1,0:T(8,128)(2,1)}), bf16[1024,2048]{1,0:T(8,128)(2,1)}) %all-gather.14.cloned.1.call-update) | async-done | bytes 4194320 | tf_op jit(solution)/shard_map/all_gather | solution.py:89
  268.7 14.5 %convolution_convert_fusion = bf16[512,2048]{1,0:T(8,128)(2,1)} fusion(bf16[1024,2048]{1,0:T(8,128)(2,1)} %all-gather.14.cloned.1.call-done, f32[64,8,8,128]{3,2,1,0:T(8,128)} %bitcast.51, bf16[2048,1024]{1,0:T(8,128)(2,1)} %all-gather.10.cloned.1.call-done, bf16[512,2048]{1,0:T(8,128)(2,1)S(1)} %copy-done, f32[2048]{0:T(1024)S(1)} %convert_element_type.144, ...), kind=kOutput, calls=%fused_computation.23 | convolution fusion | flops 4334813184 | bytes 14690304 | tf_op jit(solution)/shard_map/dot_general | solution.py:15
  285.3 2.1 all_gather.32
  287.5 15.4 %all-reduce.5.cloned.1.call-done = bf16[512,2048]{1,0:T(8,128)(2,1)} async-done(((bf16[512,2048]{1,0:T(8,128)(2,1)}), bf16[512,2048]{1,0:T(8,128)(2,1)}) %all-reduce.5.cloned.1.call-update) | async-done | bytes 2097168 | tf_op jit(solution)/shard_map/psum | solution.py:91
  302.8 3.9 fusion
  306.8 112.2 %all-gather.16.cloned.1.call-done = bf16[2048,2048]{1,0:T(8,128)(2,1)} async-done(((bf16[128,2048]{1,0:T(8,128)(2,1)}), bf16[2048,2048]{1,0:T(8,128)(2,1)}) %all-gather.16.cloned.1.call-update) | async-done | bytes 8388624 | tf_op jit(solution)/shard_map/all_gather | solution.py:96
  419.0 10.0 %convolution_convert_fusion.3 = bf16[512,2048]{1,0:T(8,128)(2,1)} fusion(bf16[2048,2048]{1,0:T(8,128)(2,1)} %all-gather.16.cloned.1.call-done, bf16[512,2048]{1,0:T(8,128)(2,1)} %get-tuple-element.10, f32[2048]{0:T(1024)S(1)} %convert_element_type.155, f32[512]{0:T(512)S(1)} %add_rsqrt_fusion), kind=kOutput, calls=%fused_computation.26 | convolution fusion | flops 4300210176 | bytes 12593152 | tf_op jit(solution)/shard_map/dot_general | solution.py:15
  429.0 103.2 %all-gather.18.cloned.1.call-done = bf16[2048,2048]{1,0:T(8,128)(2,1)} async-done(((bf16[128,2048]{1,0:T(8,128)(2,1)}), bf16[2048,2048]{1,0:T(8,128)(2,1)}) %all-gather.18.cloned.1.call-update) | async-done | bytes 8388624 | tf_op jit(solution)/shard_map/all_gather | solution.py:97
  532.2 8.4 %convolution_convert_fusion.2 = bf16[512,2048]{1,0:T(8,128)(2,1)S(1)} fusion(bf16[2048,2048]{1,0:T(8,128)(2,1)} %all-gather.18.cloned.1.call-done, bf16[512,2048]{1,0:T(8,128)(2,1)S(1)} %copy-done.1, f32[2048]{0:T(1024)S(1)} %convert_element_type.155, f32[512]{0:T(512)S(1)} %add_rsqrt_fusion), kind=kOutput, calls=%fused_computation.25 | convolution fusion | flops 4300210176 | bytes 12593152 | tf_op jit(solution)/shard_map/dot_general | solution.py:15
  540.7 3.0 multiply_add_fusion
  543.7 2.6 fusion.7
  546.3 128.7 %all-gather.20.cloned.1.call-done = bf16[2048,2048]{1,0:T(8,128)(2,1)} async-done(((bf16[2048,128]{1,0:T(8,128)(2,1)}), bf16[2048,2048]{1,0:T(8,128)(2,1)}) %all-gather.20.cloned.1.call-update) | async-done | bytes 8388624 | tf_op jit(solution)/shard_map/all_gather | solution.py:104
  675.0 9.9 %convolution_convert_fusion.1 = bf16[512,2048]{1,0:T(8,128)(2,1)} fusion(bf16[512,2048]{1,0:T(8,128)(2,1)} %fusion.7, bf16[2048,2048]{1,0:T(8,128)(2,1)} %all-gather.20.cloned.1.call-done), kind=kOutput, calls=%fused_computation.24 | convolution fusion | flops 4296015872 | bytes 12582912 | tf_op jit(solution)/shard_map/dot_general | solution.py:15
  684.9 8.0 %reduce-scatter.2.cloned.1.call-done = bf16[512,1024]{1,0:T(8,128)(2,1)} async-done(((bf16[512,2048]{1,0:T(8,128)(2,1)}), bf16[512,1024]{1,0:T(8,128)(2,1)}) %reduce-scatter.2.cloned.1.call-update) | async-done | bytes 1048592 | tf_op jit(solution)/shard_map/reduce_scatter | solution.py:108
  692.9 2.6 add_convert_fusion
  (46 shorter events, 9.2 us)
Async XLA Ops:
  6.5 15.7 %all-gather.8.cloned.1.call-start = ((), (), s32[]{:S(2)}) async-start(), calls=%async_computation.1 | async-start | bytes 3145728 | tf_op jit(solution)/shard_map/all_gather | solution.py:55
  7.3 94.5 %all-gather.12.cloned.1.call-start = ((), (), s32[]{:S(2)}) async-start(), calls=%async_computation.3 | async-start | bytes 4456448 | tf_op jit(solution)/shard_map/all_gather | solution.py:63
  8.0 170.8 %all-gather.10.cloned.1.call-start = ((), (), s32[]{:S(2)}) async-start(), calls=%async_computation.2 | async-start | bytes 4456448 | tf_op jit(solution)/shard_map/all_gather | solution.py:62
  8.7 259.9 %all-gather.14.cloned.1.call-start = ((), (), s32[]{:S(2)}) async-start(), calls=%async_computation.4 | async-start | bytes 4456448 | tf_op jit(solution)/shard_map/all_gather | solution.py:89
  9.3 293.5 %all-reduce.5.cloned.1.call-start = ((), (), s32[]{:S(2)}) async-start(), calls=%async_computation.5 | async-start | bytes 4194304 | tf_op jit(solution)/shard_map/psum | solution.py:91
  22.2 79.6 %copy-start = (bf16[512,2048]{1,0:T(8,128)(2,1)S(1)}, bf16[512,2048]{1,0:T(8,128)(2,1)}, u32[]{:S(2)}) copy-start(bf16[512,2048]{1,0:T(8,128)(2,1)} %all-gather.8.cloned.1.call-done) | copy-start | bytes 6291460
  114.1 2.4 copy-start.3
  283.2 2.2 copy-start.6
  283.2 4.2 copy-start.4
  283.2 4.3 copy-start.5
  283.2 135.8 %all-gather.16.cloned.1.call-start = ((), (), s32[]{:S(2)}) async-start(), calls=%async_computation.6 | async-start | bytes 8912896 | tf_op jit(solution)/shard_map/all_gather | solution.py:96
  283.8 248.4 %all-gather.18.cloned.1.call-start = ((), (), s32[]{:S(2)}) async-start(), calls=%async_computation.7 | async-start | bytes 8912896 | tf_op jit(solution)/shard_map/all_gather | solution.py:97
  284.5 390.4 %all-gather.20.cloned.1.call-start = ((), (), s32[]{:S(2)}) async-start(), calls=%async_computation.8 | async-start | bytes 8912896 | tf_op jit(solution)/shard_map/all_gather | solution.py:104
  285.3 407.6 %reduce-scatter.2.cloned.1.call-start = ((), (), s32[]{:S(2)}) async-start(), calls=%async_computation.9 | async-start | bytes 3145728 | tf_op jit(solution)/shard_map/reduce_scatter | solution.py:108
  419.0 113.3 %copy-start.1 = (bf16[512,2048]{1,0:T(8,128)(2,1)S(1)}, bf16[512,2048]{1,0:T(8,128)(2,1)}, u32[]{:S(2)}) copy-start(bf16[512,2048]{1,0:T(8,128)(2,1)} %get-tuple-element.10) | copy-start | bytes 6291460
  532.2 8.4 %copy-start.2 = (bf16[512,2048]{1,0:T(8,128)(2,1)S(1)}, bf16[512,2048]{1,0:T(8,128)(2,1)}, u32[]{:S(2)}) copy-start(bf16[512,2048]{1,0:T(8,128)(2,1)} %convolution_convert_fusion.3) | copy-start | bytes 6291460
Sparse Core Ops, SparseCore 0:
  8.9 13.2 all-gather.7
  25.0 76.7 all-gather.11
  104.5 74.1 all-gather.9
  181.3 87.3 all-gather.13
  283.3 19.4 all-reduce.4
  305.5 113.4 all-gather.15
  421.7 110.4 all-gather.17
  534.9 139.9 all-gather.19
  685.0 7.7 reduce-scatter.1
where the time goes:
time: 702 us
  waiting for transfers between devices  605 us (86%)
  matrix products  54.3 us (8%)
  other arithmetic  18.7 us (3%)
  between operations  13.3 us (2%)
    all_gather x1, waiting for transfers between devices, on_device(): whole_down = lax.all_gather(proj_down, 'fs', axis=1, tiled=True)  129 us
    all_gather x1, waiting for transfers between devices, on_device(): lax.all_gather(ffn_gate, 'fs', axis=0, tiled=True)  112 us
    all_gather x1, waiting for transfers between devices, on_device(): lax.all_gather(ffn_value, 'fs', axis=0, tiled=True)  103 us
    all_gather x1, waiting for transfers between devices, on_device(): whole_out = lax.all_gather(proj_out, 'fs', axis=1, tiled=True)  89.9 us
    all_gather x1, waiting for transfers between devices, on_device(): lax.all_gather(proj_v, 'fs', axis=0, tiled=True)  77.3 us
    all_gather x1, waiting for transfers between devices, on_device(): lax.all_gather(proj_u, 'fs', axis=0, tiled=True)  57.5 us
    dot_general x5, matrix products, matmul(): return jnp.dot(operand, matrix, preferred_element_type=jnp.float32)  52.5 us
    psum x1, waiting for transfers between devices, on_device(): lax.psum(partial_value.astype(jnp.bfloat16), 'tp').astype(jnp.float32)  15.4 us
  transfers between devices with their start and end apart: 9, of which 9 were waited for; matrix products, arithmetic and copies ran while one was open for 7% of the time, Pallas kernels for 0%

commit v1 on v0

--- a/solution.py
+++ b/solution.py
@@ -101,7 +101,9 @@
     conv_g = causal_taps(pre_gate.astype(jnp.bfloat16), conv_gate)
     conv_v = causal_taps(pre_value.astype(jnp.bfloat16), conv_value)
     hidden = (jax.nn.silu(conv_g) * conv_v).astype(jnp.bfloat16)
-    whole_down = lax.all_gather(proj_down, "fs", axis=1, tiled=True)
+    whole_down = jnp.concatenate(
+        lax.all_to_all(jnp.stack([proj_down] * lax.axis_size("fs")), "fs", 0, 0), axis=1
+    )
     partial_two = matmul(hidden, whole_down)
     return (
         stream.astype(jnp.float32)

time: 702 us -> 706 us (level)
    all_gather x1, waiting for transfers between devices: 112 us -> 244 us  [on_device(): lax.all_gather(ffn_gate, 'fs', axis=0, tiled=True)]
    all_gather x1 -> x0, waiting for transfers between devices: 129 us -> none  [on_device(): whole_down = lax.all_gather(proj_down, 'fs', axis=1, tiled=True)]
    all_gather x1, waiting for transfers between devices: 89.9 us -> 70.6 us  [on_device(): whole_out = lax.all_gather(proj_out, 'fs', axis=1, tiled=True)]
    all_gather x1, waiting for transfers between devices: 57.5 us -> 76.4 us  [on_device(): lax.all_gather(proj_u, 'fs', axis=0, tiled=True)]
    psum x1, waiting for transfers between devices: 15.4 us -> 6.85 us  [on_device(): lax.psum(partial_value.astype(jnp.bfloat16), 'tp').astype(jnp.float32)]
  transfers between devices with their start and end apart: 9 -> 9, of which waited for: 9 -> 8; matrix products, arithmetic and copies ran while one was open for 7% -> 8% of each run, Pallas kernels for 0% -> 0%
where the time goes in v1:
time: 706 us
  waiting for transfers between devices  600 us (85%)
  matrix products  54.3 us (8%)
  other arithmetic  17.9 us (3%)
  between operations  13.6 us (2%)
  local copies, waits for them, and re-layouts  8.04 us (1%)
    all_gather x1, waiting for transfers between devices, on_device(): lax.all_gather(ffn_gate, 'fs', axis=0, tiled=True)  244 us
    all_gather x1, waiting for transfers between devices, on_device(): lax.all_gather(ffn_value, 'fs', axis=0, tiled=True)  104 us
    all_gather x1, waiting for transfers between devices, on_device(): lax.all_gather(proj_v, 'fs', axis=0, tiled=True)  77.3 us
    all_gather x1, waiting for transfers between devices, on_device(): lax.all_gather(proj_u, 'fs', axis=0, tiled=True)  76.4 us
    all_gather x1, waiting for transfers between devices, on_device(): whole_out = lax.all_gather(proj_out, 'fs', axis=1, tiled=True)  70.6 us
    dot_general x5, matrix products, matmul(): return jnp.dot(operand, matrix, preferred_element_type=jnp.float32)  52.4 us
  transfers between devices with their start and end apart: 9, of which 8 were waited for; matrix products, arithmetic and copies ran while one was open for 8% of the time, Pallas kernels for 0%

profile of v1, /device:TPU:0, one launch (start us, length us, event | category | flops | bytes accessed | tf_op | source)
XLA Modules:
  0.0 705.7 jit_solution(10779843324681756556)
XLA Ops:
  9.4 2.1 all_gather.25
  13.6 8.6 %all-gather.7.cloned.1.call-done = bf16[512,2048]{1,0:T(8,128)(2,1)} async-done(((bf16[512,1024]{1,0:T(8,128)(2,1)}), bf16[512,2048]{1,0:T(8,128)(2,1)}) %all-gather.7.cloned.1.call-update) | async-done | bytes 2097168 | tf_op jit(solution)/shard_map/all_gather | solution.py:55
  22.2 2.2 fusion.3
  24.4 77.3 %all-gather.11.cloned.1.call-done = bf16[2048,1024]{1,0:T(8,128)(2,1)} async-done(((bf16[128,1024]{1,0:T(8,128)(2,1)}), bf16[2048,1024]{1,0:T(8,128)(2,1)}) %all-gather.11.cloned.1.call-update) | async-done | bytes 4194320 | tf_op jit(solution)/shard_map/all_gather | solution.py:63
  101.8 9.6 %fusion.107 = (f32[512]{0:T(512)S(1)}, f32[512]{0:T(512)S(1)}, f32[512,1024]{1,0:T(8,128)}) fusion(bf16[2048,1024]{1,0:T(8,128)(2,1)} %all-gather.11.cloned.1.call-done, bf16[512,2048]{1,0:T(8,128)(2,1)S(1)} %copy-done, f32[2048]{0:T(1024)S(1)} %convert_element_type.147, f32[512]{0:T(512)S(1)} %add_rsqrt_fusion.2), kind=kOutput, calls=%fused_computation.144 | convolution fusion | flops 2186804224 | bytes 8402944 | tf_op jit(solution)/shard_map/dot_general | solution.py:15
  111.4 2.6 all-reduce.2
  114.0 2.1 fusion.28
  118.3 3.0 copy.22
  121.2 70.6 %all-gather.13.cloned.1.call-done = bf16[1024,2048]{1,0:T(8,128)(2,1)} async-done(((bf16[1024,128]{1,0:T(8,128)(2,1)}), bf16[1024,2048]{1,0:T(8,128)(2,1)}) %all-gather.13.cloned.1.call-update) | async-done | bytes 4194320 | tf_op jit(solution)/shard_map/all_gather | solution.py:89
  191.8 76.4 %all-gather.9.cloned.1.call-done = bf16[2048,1024]{1,0:T(8,128)(2,1)} async-done(((bf16[128,1024]{1,0:T(8,128)(2,1)}), bf16[2048,1024]{1,0:T(8,128)(2,1)}) %all-gather.9.cloned.1.call-update) | async-done | bytes 4194320 | tf_op jit(solution)/shard_map/all_gather | solution.py:62
  268.3 14.4 %convolution_convert_fusion = bf16[512,2048]{1,0:T(8,128)(2,1)} fusion(bf16[1024,2048]{1,0:T(8,128)(2,1)} %all-gather.13.cloned.1.call-done, f32[64,8,8,128]{3,2,1,0:T(8,128)} %bitcast.41, bf16[2048,1024]{1,0:T(8,128)(2,1)} %all-gather.9.cloned.1.call-done, bf16[512,2048]{1,0:T(8,128)(2,1)S(1)} %copy-done, f32[2048]{0:T(1024)S(1)} %convert_element_type.147, ...), kind=kOutput, calls=%fused_computation.15 | convolution fusion | flops 4334813184 | bytes 14690304 | tf_op jit(solution)/shard_map/dot_general | solution.py:15
  284.3 4.6 stack.2
  288.9 4.9 all-to-all-start
  293.8 2.1 all_gather.29
  295.9 6.8 all-reduce.5.cloned.1.call-done
  302.8 3.9 fusion
  306.7 244.2 %all-gather.15.cloned.1.call-done = bf16[2048,2048]{1,0:T(8,128)(2,1)} async-done(((bf16[128,2048]{1,0:T(8,128)(2,1)}), bf16[2048,2048]{1,0:T(8,128)(2,1)}) %all-gather.15.cloned.1.call-update) | async-done | bytes 8388624 | tf_op jit(solution)/shard_map/all_gather | solution.py:96
  550.9 10.1 %convolution_convert_fusion.3 = bf16[512,2048]{1,0:T(8,128)(2,1)} fusion(bf16[2048,2048]{1,0:T(8,128)(2,1)} %all-gather.15.cloned.1.call-done, bf16[512,2048]{1,0:T(8,128)(2,1)} %get-tuple-element.10, f32[2048]{0:T(1024)S(1)} %convert_element_type.158, f32[512]{0:T(512)S(1)} %add_rsqrt_fusion), kind=kOutput, calls=%fused_computation.18 | convolution fusion | flops 4300210176 | bytes 12593152 | tf_op jit(solution)/shard_map/dot_general | solution.py:15
  560.9 104.1 %all-gather.17.cloned.1.call-done = bf16[2048,2048]{1,0:T(8,128)(2,1)} async-done(((bf16[128,2048]{1,0:T(8,128)(2,1)}), bf16[2048,2048]{1,0:T(8,128)(2,1)}) %all-gather.17.cloned.1.call-update) | async-done | bytes 8388624 | tf_op jit(solution)/shard_map/all_gather | solution.py:97
  665.0 8.4 %convolution_convert_fusion.2 = bf16[512,2048]{1,0:T(8,128)(2,1)S(1)} fusion(bf16[2048,2048]{1,0:T(8,128)(2,1)} %all-gather.17.cloned.1.call-done, bf16[512,2048]{1,0:T(8,128)(2,1)S(1)} %copy-done.1, f32[2048]{0:T(1024)S(1)} %convert_element_type.158, f32[512]{0:T(512)S(1)} %add_rsqrt_fusion), kind=kOutput, calls=%fused_computation.17 | convolution fusion | flops 4300210176 | bytes 12593152 | tf_op jit(solution)/shard_map/dot_general | solution.py:15
  673.4 4.9 multiply_convert_fusion
  678.4 9.9 %convolution_convert_fusion.1 = bf16[512,2048]{1,0:T(8,128)(2,1)} fusion(bf16[512,2048]{1,0:T(8,128)(2,1)} %bitcast.39, bf16[2048,2048]{0,1:T(8,128)(2,1)} %bitcast.14), kind=kOutput, calls=%fused_computation.16 | convolution fusion | flops 4296015872 | bytes 12582912 | tf_op jit(solution)/shard_map/dot_general | solution.py:15
  688.3 8.0 %reduce-scatter.2.cloned.1.call-done = bf16[512,1024]{1,0:T(8,128)(2,1)} async-done(((bf16[512,2048]{1,0:T(8,128)(2,1)}), bf16[512,1024]{1,0:T(8,128)(2,1)}) %reduce-scatter.2.cloned.1.call-update) | async-done | bytes 1048592 | tf_op jit(solution)/shard_map/reduce_scatter | solution.py:110
  696.3 2.6 add_convert_fusion
  (48 shorter events, 8.7 us)
Async XLA Ops:
  6.5 15.7 %all-gather.7.cloned.1.call-start = ((), (), s32[]{:S(2)}) async-start(), calls=%async_computation.2 | async-start | bytes 3145728 | tf_op jit(solution)/shard_map/all_gather | solution.py:55
  7.3 94.5 %all-gather.11.cloned.1.call-start = ((), (), s32[]{:S(2)}) async-start(), calls=%async_computation.4 | async-start | bytes 4456448 | tf_op jit(solution)/shard_map/all_gather | solution.py:63
  8.0 183.8 %all-gather.13.cloned.1.call-start = ((), (), s32[]{:S(2)}) async-start(), calls=%async_computation.5 | async-start | bytes 4456448 | tf_op jit(solution)/shard_map/all_gather | solution.py:89
  8.7 259.5 %all-gather.9.cloned.1.call-start = ((), (), s32[]{:S(2)}) async-start(), calls=%async_computation.3 | async-start | bytes 4456448 | tf_op jit(solution)/shard_map/all_gather | solution.py:62
  9.3 293.5 %all-reduce.5.cloned.1.call-start = ((), (), s32[]{:S(2)}) async-start(), calls=%async_computation.6 | async-start | bytes 4194304 | tf_op jit(solution)/shard_map/psum | solution.py:91
  22.2 79.6 %copy-start = (bf16[512,2048]{1,0:T(8,128)(2,1)S(1)}, bf16[512,2048]{1,0:T(8,128)(2,1)}, u32[]{:S(2)}) copy-start(bf16[512,2048]{1,0:T(8,128)(2,1)} %all-gather.7.cloned.1.call-done) | copy-start | bytes 6291460
  114.0 2.4 copy-start.4
  282.7 1.4 copy-start.3
  282.7 268.1 %all-gather.15.cloned.1.call-start = ((), (), s32[]{:S(2)}) async-start(), calls=%async_computation.7 | async-start | bytes 8912896 | tf_op jit(solution)/shard_map/all_gather | solution.py:96
  283.3 381.7 %all-gather.17.cloned.1.call-start = ((), (), s32[]{:S(2)}) async-start(), calls=%async_computation.8 | async-start | bytes 8912896 | tf_op jit(solution)/shard_map/all_gather | solution.py:97
  288.9 5.0 copy-start.7
  288.9 7.0 copy-start.5
  288.9 7.0 copy-start.6
  288.9 389.5 %all-to-all-start = ((bf16[16,2048,128]{1,2,0:T(8,128)(2,1)}), bf16[16,2048,128]{1,2,0:T(8,128)(2,1)}, u32[]{:S(2)}, u32[]{:S(2)}) async-start(bf16[16,2048,128]{1,2,0:T(8,128)(2,1)} %stack.2), calls=%async_computation | async-start | bytes 16777216 | tf_op jit(solution)/shard_map/all_to_all | solution.py:105
  293.8 402.5 %reduce-scatter.2.cloned.1.call-start = ((), (), s32[]{:S(2)}) async-start(), calls=%async_computation.9 | async-start | bytes 3145728 | tf_op jit(solution)/shard_map/reduce_scatter | solution.py:110
  550.8 114.2 %copy-start.1 = (bf16[512,2048]{1,0:T(8,128)(2,1)S(1)}, bf16[512,2048]{1,0:T(8,128)(2,1)}, u32[]{:S(2)}) copy-start(bf16[512,2048]{1,0:T(8,128)(2,1)} %get-tuple-element.10) | copy-start | bytes 6291460
  665.0 8.4 %copy-start.2 = (bf16[512,2048]{1,0:T(8,128)(2,1)S(1)}, bf16[512,2048]{1,0:T(8,128)(2,1)}, u32[]{:S(2)}) copy-start(bf16[512,2048]{1,0:T(8,128)(2,1)} %convolution_convert_fusion.3) | copy-start | bytes 6291460
Sparse Core Ops, SparseCore 0:
  8.9 13.2 all-gather.6
  25.0 76.7 all-gather.10
  104.5 87.3 all-gather.12
  194.5 73.7 all-gather.8
  282.8 19.9 all-reduce.4
  305.4 245.3 all-gather.14
  553.6 111.3 all-gather.16
  688.4 7.7 reduce-scatter.1
